TPU v7x, 32 devices: a whole 2x2x4 slice. The times are simulated.
32 devices in a mesh: grp: 2 (over y), sp: 4 (over z), tp: 4 (over x, core).
Axes of the slice: x: 2, y: 2, z: 4, core: 2. Of those that a mesh axis runs over, the one named last changes fastest.
Arguments:
- queries: bfloat16 [4096, 1024], P(('grp', 'sp'), 'tp'), parts along dimension 0, may hold values from -120 to 120
- keys: bfloat16 [4096, 256], P(('grp', 'sp')), parts along dimension 0, may hold values from -6 to 6
- values: bfloat16 [4096, 256], P(('grp', 'sp')), parts along dimension 0, may hold values from -6 to 6
- sink: float32 [8], P('tp'), may hold values from 1 to 5
- resid: bfloat16 [4096, 2048], P(('grp', 'sp')), parts along dimension 0, may hold values from -100 to 100
- out_proj: bfloat16 [1024, 2048], P(None, 'tp'), may hold values from -1.5 to 1.5
- norm_gain: float32 [2048], replicated, may hold values from 0.1 to 1.9
- w_gate: bfloat16 [2048, 6144], P('sp', 'tp'), may hold values from -0.125 to 0.125
- w_up: bfloat16 [2048, 6144], P('sp', 'tp'), may hold values from -0.125 to 0.125
- conv_w: float32 [3, 6144], P(None, 'tp'), may hold values from -3 to 3
- conv_b: float32 [6144], P('tp'), may hold values from -3 to 3
- w_down: bfloat16 [6144, 2048], P('tp', 'sp'), may hold values from -0.21875 to 0.21875
Outputs:
- layer_out: bfloat16 [4096, 2048], P(('grp', 'sp'), 'tp'), parts along dimension 0
There are 2 independent parts, one for each index of `grp`. A program takes and returns all parts, laid end to end along the dimension named above; an argument that names none is the same for every part. Nothing has to cross between parts.
All inputs are finite; a program needn't handle non-finite values.
Results may differ from a plain program's by a relative error of at most 0.015.
Values may be sent and summed in bfloat16 or wider, within the bound.
A program may use at most 64 MiB of HBM per device.

v0:
```python
import jax
import jax.numpy as jnp
from jax import lax
from jax.sharding import PartitionSpec as P

H = 8
KVH = 2
HD = 128
WINDOW = 128
CONV = 3


def with_halo(cells, sides, width):
    for axis, dim in sides:
        count = lax.axis_size(axis)
        ends = count - 1
        head = lax.slice_in_dim(cells, 0, width, axis=dim)
        tail = lax.slice_in_dim(cells, cells.shape[dim] - width, cells.shape[dim], axis=dim)
        cells = jnp.concatenate(
            [
                lax.ppermute(tail, axis, [(i, (i + 1) % count) for i in range(ends)]),
                cells,
                lax.ppermute(head, axis, [((i + 1) % count, i) for i in range(ends)]),
            ],
            axis=dim,
        )
    return cells


def shards(
    queries, keys, values, sink, resid, out_proj, norm_gain, w_gate, w_up, conv_w, conv_b, w_down
):
    tokens = queries.shape[0]
    width = resid.shape[1]
    heads_here = sink.shape[0]
    group = H // KVH
    scale = HD ** (-0.5)
    first_head = lax.axis_index("tp") * heads_here
    kv_head = first_head // group
    own_keys = lax.dynamic_slice_in_dim(keys, kv_head * HD, HD, 1)
    own_values = lax.dynamic_slice_in_dim(values, kv_head * HD, HD, 1)
    extended = with_halo(jnp.stack([own_keys, own_values]), (("sp", 1),), WINDOW)
    ext_keys = extended[0]
    ext_values = extended[1]
    span = tokens + 2 * WINDOW
    q_heads = queries.reshape(tokens, heads_here, HD)
    scores = (
        jnp.einsum("qhd,kd->hqk", q_heads, ext_keys, preferred_element_type=jnp.float32) * scale
    )
    offset = lax.axis_index("sp") * tokens
    q_pos = offset + jnp.arange(tokens, dtype=jnp.int32)[:, None]
    k_pos = offset - WINDOW + jnp.arange(span, dtype=jnp.int32)[None, :]
    seq_total = tokens * lax.axis_size("sp")
    valid = (jnp.abs(q_pos - k_pos) <= WINDOW) & (k_pos >= 0) & (k_pos < seq_total)
    scores = jnp.where(valid[None], scores, jnp.float32(-1e30))
    sink_col = sink[:, None]
    top = jnp.maximum(jnp.max(scores, axis=-1), sink_col)
    expo = jnp.exp(scores - top[..., None])
    total = jnp.sum(expo, axis=-1) + jnp.exp(sink_col - top)
    weights = (expo / total[..., None]).astype(jnp.bfloat16)
    heads_out = jnp.einsum("hqk,kd->qhd", weights, ext_values, preferred_element_type=jnp.float32)
    heads_out = heads_out.astype(jnp.bfloat16).reshape(tokens, heads_here * HD)
    all_heads = lax.all_gather(heads_out, "tp", axis=1, tiled=True)
    cols = width // lax.axis_size("tp")
    col_start = lax.axis_index("tp") * cols
    full_proj = lax.all_gather(out_proj, "tp", axis=1, tiled=True)
    summed = resid.astype(jnp.float32) + jnp.dot(
        all_heads, full_proj, preferred_element_type=jnp.float32
    )
    mean = jnp.mean(summed, axis=-1, keepdims=True)
    msq = jnp.mean(summed * summed, axis=-1, keepdims=True)
    normed_full = ((summed - mean) * lax.rsqrt(msq - mean * mean + 1e-05) * norm_gain).astype(
        jnp.bfloat16
    )
    normed_own = lax.dynamic_slice_in_dim(normed_full, col_start, cols, 1)
    gate_acc = jnp.dot(
        normed_full,
        lax.all_gather(w_gate, "sp", axis=0, tiled=True),
        preferred_element_type=jnp.float32,
    )
    up_acc = jnp.dot(
        normed_full,
        lax.all_gather(w_up, "sp", axis=0, tiled=True),
        preferred_element_type=jnp.float32,
    )
    gate_pre = gate_acc.astype(jnp.bfloat16)
    up_part = up_acc.astype(jnp.bfloat16)
    padded = with_halo(gate_pre, (("sp", 0),), CONV // 2)
    conv = conv_b
    for tap in range(CONV):
        conv = conv + padded[tap : tap + tokens].astype(jnp.float32) * conv_w[tap]
    act = (jax.nn.silu(conv) * up_part.astype(jnp.float32)).astype(jnp.bfloat16)
    terms = jnp.dot(
        act, lax.all_gather(w_down, "sp", axis=1, tiled=True), preferred_element_type=jnp.float32
    )
    ffn_own = lax.psum_scatter(
        terms.astype(jnp.bfloat16), "tp", scatter_dimension=1, tiled=True
    ).astype(jnp.float32)
    return (normed_own.astype(jnp.float32) + ffn_own).astype(jnp.bfloat16)


def solution(mesh):
    return jax.shard_map(
        shards,
        mesh=mesh,
        in_specs=(
            P(("grp", "sp"), "tp"),
            P(("grp", "sp"), None),
            P(("grp", "sp"), None),
            P("tp"),
            P(("grp", "sp"), None),
            P(None, "tp"),
            P(),
            P("sp", "tp"),
            P("sp", "tp"),
            P(None, "tp"),
            P("tp"),
            P("tp", "sp"),
        ),
        out_specs=P(("grp", "sp"), "tp"),
        check_vma=False,
    )
```

profile of v0, /device:TPU:0, one launch (start us, length us, event | category | flops | bytes accessed | tf_op | source)
XLA Modules:
  0.0 476.0 jit_solution(9016852230966235995)
XLA Ops:
  6.5 1.0 dynamic-slice_bitcast_fusion
  7.6 5.0 %collective-permute-start = (bf16[2,128,128]{2,1,0:T(8,128)(2,1)S(1)}, bf16[2,128,128]{2,1,0:T(8,128)(2,1)S(1)}, u32[]{:S(2)}, u32[]{:S(2)}) collective-permute-start(bf16[2,128,128]{2,1,0:T(8,128)(2,1)S(1)} %get-tuple-element.12), channel_id=1, source_target_pairs={{0,4},{4,8},{8,12},{1,5},{5,9},{9,13},{2,6},{6,10},{10,14},{3,7},{... | collective-permute-start | bytes 196616 | tf_op jit(solution)/shard_map/ppermute | solution.py:21
  12.6 1.3 collective-permute-start.1
  13.9 0.8 fusion.10
  14.7 4.0 collective-permute-done.1
  18.8 0.8 fusion.1
  19.6 0.7 fusion
  20.4 1.9 fusion.12
  22.3 0.7 all-gather.8.cloned.1.call-update
  23.1 0.7 all-gather.10.cloned.1.call-update
  24.4 0.5 all-gather.14.cloned.1.call-update
  25.0 14.4 %all-gather.6.cloned.1.call-done = bf16[512,1024]{0,1:T(8,128)(2,1)} async-done(((bf16[512,256]{0,1:T(8,128)(2,1)}), bf16[512,1024]{0,1:T(8,128)(2,1)}) %all-gather.6.cloned.1.call-update) | async-done | bytes 1048592 | tf_op jit(solution)/shard_map/all_gather | solution.py:63
  39.4 36.0 %all-gather.8.cloned.1.call-done = bf16[1024,2048]{1,0:T(8,128)(2,1)} async-done(((bf16[1024,512]{1,0:T(8,128)(2,1)}), bf16[1024,2048]{1,0:T(8,128)(2,1)}) %all-gather.8.cloned.1.call-update) | async-done | bytes 4194320 | tf_op jit(solution)/shard_map/all_gather | solution.py:66
  75.4 5.4 %fusion.22 = (f32[512]{0:T(512)S(1)}, f32[512]{0:T(512)S(1)}, f32[512,2048]{1,0:T(8,128)S(1)}) fusion(bf16[512,1024]{0,1:T(8,128)(2,1)} %all-gather.6.cloned.1.call-done, bf16[1024,2048]{1,0:T(8,128)(2,1)} %all-gather.8.cloned.1.call-done, bf16[512,2048]{1,0:T(8,128)(2,1)S(1)} %copy-done.5), kind=kOutput, calls=%fused_computation.52 | convolution fusion | flops 2152725504 | bytes 11538432 | tf_op jit(solution)/shard_map/dot_general | solution.py:67
  80.8 0.6 multiply_convert_fusion
  81.5 110.9 %all-gather.10.cloned.1.call-done = bf16[2048,1536]{1,0:T(8,128)(2,1)} async-done(((bf16[512,1536]{1,0:T(8,128)(2,1)}), bf16[2048,1536]{1,0:T(8,128)(2,1)}) %all-gather.10.cloned.1.call-update) | async-done | bytes 6291472 | tf_op jit(solution)/shard_map/all_gather | solution.py:78
  192.4 6.2 %convolution_convert_fusion.2 = bf16[512,1536]{1,0:T(8,128)(2,1)S(1)} fusion(bf16[512,2048]{1,0:T(8,128)(2,1)S(1)} %multiply_convert_fusion, bf16[2048,1536]{1,0:T(8,128)(2,1)} %all-gather.10.cloned.1.call-done), kind=kOutput, calls=%fused_computation.9 | convolution fusion | flops 3222011904 | bytes 9961472 | tf_op jit(solution)/shard_map/dot_general | solution.py:76
  198.6 1.3 collective-permute-start.2
  199.9 1.5 collective-permute-start.3
  201.5 105.9 %all-gather.12.cloned.1.call-done = bf16[2048,1536]{1,0:T(8,128)(2,1)} async-done(((bf16[512,1536]{1,0:T(8,128)(2,1)}), bf16[2048,1536]{1,0:T(8,128)(2,1)}) %all-gather.12.cloned.1.call-update) | async-done | bytes 6291472 | tf_op jit(solution)/shard_map/all_gather | solution.py:83
  307.4 114.9 %all-gather.14.cloned.1.call-done = bf16[1536,2048]{1,0:T(8,128)(2,1)} async-done(((bf16[1536,512]{1,0:T(8,128)(2,1)}), bf16[1536,2048]{1,0:T(8,128)(2,1)}) %all-gather.14.cloned.1.call-update) | async-done | bytes 6291472 | tf_op jit(solution)/shard_map/all_gather | solution.py:94
  422.3 15.3 %convolution_convert_fusion = bf16[512,2048]{1,0:T(8,128)(2,1)} fusion(bf16[1536,2048]{1,0:T(8,128)(2,1)} %all-gather.14.cloned.1.call-done, bf16[512,1536]{1,0:T(8,128)(2,1)} %copy-done.4, bf16[1,1536]{1,0:T(2,128)(2,1)S(1)} %collective-permute-done.3, bf16[1,1536]{1,0:T(2,128)(2,1)S(1)} %collective-permute-done.2, f32[1536]{0:T(1024)S(1)} %get-tuple-element.8, ...), kind=kOutput, calls=%fused_computation.7 | convolution fusion | flops 6461587456 | bytes 18380800 | tf_op jit(solution)/shard_map/dot_general | solution.py:93
  437.6 29.5 %reduce-scatter.2.cloned.1.call-done = bf16[512,512]{1,0:T(8,128)(2,1)} async-done(((bf16[512,2048]{1,0:T(8,128)(2,1)}), bf16[512,512]{1,0:T(8,128)(2,1)}) %reduce-scatter.2.cloned.1.call-update) | async-done | bytes 524304 | tf_op jit(solution)/shard_map/reduce_scatter | solution.py:96
  467.1 2.0 add_convert_fusion
  (36 shorter events, 1.1 us)
Async XLA Ops:
  6.5 12.2 %copy-start = (bf16[512,256]{1,0:T(8,128)(2,1)S(1)}, bf16[512,256]{1,0:T(8,128)(2,1)}, u32[]{:S(2)}) copy-start(bf16[512,256]{1,0:T(8,128)(2,1)} %param.12) | copy-start | bytes 786436
  6.5 32.8 %all-gather.6.cloned.1.call-start = ((), (), s32[]{:S(2)}) async-start(), calls=%async_computation.1 | async-start | bytes 1310720 | tf_op jit(solution)/shard_map/all_gather | solution.py:63
  6.5 13.0 %copy-start.3 = (f32[2]{0:T(128)S(1)}, f32[2]{0:T(128)}, u32[]{:S(2)}) copy-start(f32[2]{0:T(128)} %param.15) | copy-start | bytes 28
  7.6 7.1 %collective-permute-start = (bf16[2,128,128]{2,1,0:T(8,128)(2,1)S(1)}, bf16[2,128,128]{2,1,0:T(8,128)(2,1)S(1)}, u32[]{:S(2)}, u32[]{:S(2)}) collective-permute-start(bf16[2,128,128]{2,1,0:T(8,128)(2,1)S(1)} %get-tuple-element.12), channel_id=1, source_target_pairs={{0,4},{4,8},{8,12},{1,5},{5,9},{9,13},{2,6},{6,10},{10,14},{3,7},{... | collective-permute-start | bytes 196616 | tf_op jit(solution)/shard_map/ppermute | solution.py:21
  12.6 6.2 %collective-permute-start.1 = (bf16[2,128,128]{2,1,0:T(8,128)(2,1)S(1)}, bf16[2,128,128]{2,1,0:T(8,128)(2,1)S(1)}, u32[]{:S(2)}, u32[]{:S(2)}) collective-permute-start(bf16[2,128,128]{2,1,0:T(8,128)(2,1)S(1)} %get-tuple-element.13), channel_id=1, source_target_pairs={{4,0},{8,4},{12,8},{5,1},{9,5},{13,9},{6,2},{10,6},{14,10},{7,3},{... | collective-permute-start | bytes 196616 | tf_op jit(solution)/shard_map/ppermute | solution.py:23
  22.3 53.2 %copy-start.5 = (bf16[512,2048]{1,0:T(8,128)(2,1)S(1)}, bf16[512,2048]{1,0:T(8,128)(2,1)}, u32[]{:S(2)}) copy-start(bf16[512,2048]{1,0:T(8,128)(2,1)} %param.16) | copy-start | bytes 6291460
  22.3 53.1 %all-gather.8.cloned.1.call-start = ((), (), s32[]{:S(2)}) async-start(), calls=%async_computation.2 | async-start | bytes 5242880 | tf_op jit(solution)/shard_map/all_gather | solution.py:66
  23.1 169.3 %all-gather.10.cloned.1.call-start = ((), (), s32[]{:S(2)}) async-start(), calls=%async_computation.3 | async-start | bytes 7864320 | tf_op jit(solution)/shard_map/all_gather | solution.py:78
  23.8 283.6 %all-gather.12.cloned.1.call-start = ((), (), s32[]{:S(2)}) async-start(), calls=%async_computation.4 | async-start | bytes 7864320 | tf_op jit(solution)/shard_map/all_gather | solution.py:83
  24.4 398.0 %all-gather.14.cloned.1.call-start = ((), (), s32[]{:S(2)}) async-start(), calls=%async_computation.5 | async-start | bytes 7864320 | tf_op jit(solution)/shard_map/all_gather | solution.py:94
  24.9 55.9 %copy-start.2 = (f32[2048]{0:T(1024)S(1)}, f32[2048]{0:T(1024)}, u32[]{:S(2)}) copy-start(f32[2048]{0:T(1024)} %param.18) | copy-start | bytes 24580
  25.0 442.2 %reduce-scatter.2.cloned.1.call-start = ((), (), s32[]{:S(2)}) async-start(), calls=%async_computation.6 | async-start | bytes 2621440 | tf_op jit(solution)/shard_map/reduce_scatter | solution.py:96
  81.5 119.9 %copy-start.1 = (f32[3,1536]{1,0:T(4,128)S(1)}, f32[3,1536]{1,0:T(4,128)}, u32[]{:S(2)}) copy-start(f32[3,1536]{1,0:T(4,128)} %param.21) | copy-start | bytes 55300
  81.5 340.9 %copy-start.6 = (f32[1536]{0:T(1024)S(1)}, f32[1536]{0:T(1024)}, u32[]{:S(2)}) copy-start(f32[1536]{0:T(1024)} %param.22) | copy-start | bytes 18436
  198.6 2.8 copy-start.4
  198.6 223.7 %collective-permute-start.2 = (bf16[1,1536]{1,0:T(2,128)(2,1)S(1)}, bf16[1,1536]{1,0:T(2,128)(2,1)S(1)}, u32[]{:S(2)}, u32[]{:S(2)}) collective-permute-start(bf16[1,1536]{1,0:T(2,128)(2,1)S(1)} %get-tuple-element.10), channel_id=1, source_target_pairs={{0,4},{4,8},{8,12},{1,5},{5,9},{9,13},{2,6},{6,10},{10,14},{3,7},{... | collective-permute-start | bytes 9224 | tf_op jit(solution)/shard_map/ppermute | solution.py:21
  199.9 222.4 %collective-permute-start.3 = (bf16[1,1536]{1,0:T(2,128)(2,1)S(1)}, bf16[1,1536]{1,0:T(2,128)(2,1)S(1)}, u32[]{:S(2)}, u32[]{:S(2)}) collective-permute-start(bf16[1,1536]{1,0:T(2,128)(2,1)S(1)} %get-tuple-element.11), channel_id=1, source_target_pairs={{4,0},{8,4},{12,8},{5,1},{9,5},{13,9},{6,2},{10,6},{14,10},{7,3},{... | collective-permute-start | bytes 9224 | tf_op jit(solution)/shard_map/ppermute | solution.py:23
Sparse Core Ops, SparseCore 0:
  22.4 16.9 all-gather.5
  40.9 34.4 all-gather.7
  77.0 115.3 all-gather.9
  193.8 113.5 all-gather.11
  308.8 113.4 all-gather.13
  437.7 29.3 reduce-scatter.1
where the time goes:
time: 476 us
  waiting for transfers between devices  418 us (88%)
  matrix products  29.4 us (6%)
  between operations  13.7 us (3%)
  starting transfers between devices  9.21 us (2%)
    all_gather x1, waiting for transfers between devices, shards(): lax.all_gather(w_down, 'sp', axis=1, tiled=True)  115 us
    all_gather x1, waiting for transfers between devices, shards(): lax.all_gather(w_gate, 'sp', axis=0, tiled=True)  111 us
    all_gather x1, waiting for transfers between devices, shards(): lax.all_gather(w_up, 'sp', axis=0, tiled=True)  106 us
    all_gather x1, waiting for transfers between devices, shards(): full_proj = lax.all_gather(out_proj, 'tp', axis=1, tiled=True)  36 us
    reduce_scatter x1, waiting for transfers between devices, shards(): lax.psum_scatter(terms.astype(jnp.bfloat16), 'tp', scatter_dimension=1, t...  29.5 us
    dot_general x1, matrix products, shards(): jnp.dot(act, lax.all_gather(w_down, 'sp', axis=1, tiled=True), preferred_...  15.3 us
    all_gather x1, waiting for transfers between devices, shards(): all_heads = lax.all_gather(heads_out, 'tp', axis=1, tiled=True)  14.4 us
  transfers between devices with their start and end apart: 10, of which 7 were waited for; matrix products, arithmetic and copies ran while one was open for 3% of the time, Pallas kernels for 0%

commit v1 on v0

--- a/solution.py
+++ b/solution.py
@@ -2,6 +2,7 @@
 import jax.numpy as jnp
 from jax import lax
 from jax.sharding import PartitionSpec as P
+from jax.lax import axis_index, axis_size, ppermute
 
 H = 8
 KVH = 2
@@ -63,7 +64,15 @@
     all_heads = lax.all_gather(heads_out, "tp", axis=1, tiled=True)
     cols = width // lax.axis_size("tp")
     col_start = lax.axis_index("tp") * cols
-    full_proj = lax.all_gather(out_proj, "tp", axis=1, tiled=True)
+    full_n = axis_size("tp")
+    pile = [(u, (u + 1) % full_n) for u in range(full_n)]
+    f_now = [None] * full_n
+    f_now[full_n - 1] = out_proj
+    for i0 in range(full_n - 2, -1, -1):
+        f_now[i0] = ppermute(f_now[i0 + 1], "tp", pile)
+    all_values = jnp.concatenate(f_now, 1)
+    z2 = (axis_index("tp") + 1) * out_proj.shape[1]
+    full_proj = jnp.roll(all_values, z2, 1)
     summed = resid.astype(jnp.float32) + jnp.dot(
         all_heads, full_proj, preferred_element_type=jnp.float32
     )

time: 476 us -> 443 us (0.931)
  waiting for transfers between devices: 418 us -> 373 us
  local copies, waits for them, and re-layouts: 1.13 us -> 12.5 us
    ppermute x0 -> x3, waiting for transfers between devices: none -> 48.4 us  [shards(): f_now[i0] = ppermute(f_now[i0 + 1], 'tp', pile)]
    all_gather x1, waiting for transfers between devices: 111 us -> 68.2 us  [shards(): lax.all_gather(w_gate, 'sp', axis=0, tiled=True)]
    all_gather x1 -> x0, waiting for transfers between devices: 36 us -> none  [shards(): full_proj = lax.all_gather(out_proj, 'tp', axis=1, tiled=True)]
    all_gather x1, waiting for transfers between devices: 14.4 us -> 0.01 us  [shards(): all_heads = lax.all_gather(heads_out, 'tp', axis=1, tiled=True)]
    unnamed x14 -> x21, local copies, waits for them, and re-layouts: 0.03 us -> 10.3 us
    all_gather x1, waiting for transfers between devices: 106 us -> 115 us  [shards(): lax.all_gather(w_up, 'sp', axis=0, tiled=True)]
    all_gather x1, waiting for transfers between devices: 115 us -> 106 us  [shards(): lax.all_gather(w_down, 'sp', axis=1, tiled=True)]
  transfers between devices with their start and end apart: 10 -> 12, of which waited for: 7 -> 8; matrix products, arithmetic and copies ran while one was open for 3% -> 6% of each run, Pallas kernels for 0% -> 0%
where the time goes in v1:
time: 443 us
  waiting for transfers between devices  373 us (84%)
  matrix products  30.2 us (7%)
  between operations  13.4 us (3%)
  local copies, waits for them, and re-layouts  12.5 us (3%)
  starting transfers between devices  9.23 us (2%)
    all_gather x1, waiting for transfers between devices, shards(): lax.all_gather(w_up, 'sp', axis=0, tiled=True)  115 us
    all_gather x1, waiting for transfers between devices, shards(): lax.all_gather(w_down, 'sp', axis=1, tiled=True)  106 us
    all_gather x1, waiting for transfers between devices, shards(): lax.all_gather(w_gate, 'sp', axis=0, tiled=True)  68.2 us
    ppermute x3, waiting for transfers between devices, shards(): f_now[i0] = ppermute(f_now[i0 + 1], 'tp', pile)  48.4 us
    reduce_scatter x1, waiting for transfers between devices, shards(): lax.psum_scatter(terms.astype(jnp.bfloat16), 'tp', scatter_dimension=1, t...  29.5 us
    dot_general x1, matrix products, shards(): jnp.dot(act, lax.all_gather(w_down, 'sp', axis=1, tiled=True), preferred_...  15.3 us
    unnamed x21, local copies, waits for them, and re-layouts  10.3 us
  transfers between devices with their start and end apart: 12, of which 8 were waited for; matrix products, arithmetic and copies ran while one was open for 6% of the time, Pallas kernels for 0%

profile of v1, /device:TPU:0, one launch (start us, length us, event | category | flops | bytes accessed | tf_op | source)
XLA Modules:
  0.0 442.8 jit_solution(9426897391186587267)
XLA Ops:
  7.6 5.0 %collective-permute-start = (bf16[2,128,128]{2,1,0:T(8,128)(2,1)S(1)}, bf16[2,128,128]{2,1,0:T(8,128)(2,1)S(1)}, u32[]{:S(2)}, u32[]{:S(2)}) collective-permute-start(bf16[2,128,128]{2,1,0:T(8,128)(2,1)S(1)} %get-tuple-element.12), channel_id=1, source_target_pairs={{0,4},{4,8},{8,12},{1,5},{5,9},{9,13},{2,6},{6,10},{10,14},{3,7},{... | collective-permute-start | bytes 196616 | tf_op jit(solution)/shard_map/ppermute | solution.py:22
  12.6 1.3 collective-permute-start.1
  14.7 4.0 collective-permute-done.1
  20.4 1.9 fusion.16
  24.5 19.8 %collective-permute-done.2 = bf16[1024,512]{1,0:T(8,128)(2,1)S(1)} collective-permute-done((bf16[1024,512]{1,0:T(8,128)(2,1)S(1)}, bf16[1024,512]{1,0:T(8,128)(2,1)S(1)}, u32[]{:S(2)}, u32[]{:S(2)}) %collective-permute-start.2) | collective-permute-done | bytes 1048608 | tf_op jit(solution)/shard_map/ppermute | solution.py:72
  44.3 14.2 %collective-permute-done.3 = bf16[1024,512]{1,0:T(8,128)(2,1)S(1)} collective-permute-done((bf16[1024,512]{1,0:T(8,128)(2,1)S(1)}, bf16[1024,512]{1,0:T(8,128)(2,1)S(1)}, u32[]{:S(2)}, u32[]{:S(2)}) %collective-permute-start.3) | collective-permute-done | bytes 1048608 | tf_op jit(solution)/shard_map/ppermute | solution.py:72
  58.5 14.3 %collective-permute-done.4 = bf16[1024,512]{1,0:T(8,128)(2,1)} collective-permute-done((bf16[1024,512]{1,0:T(8,128)(2,1)S(1)}, bf16[1024,512]{1,0:T(8,128)(2,1)}, u32[]{:S(2)}, u32[]{:S(2)}) %collective-permute-start.4) | collective-permute-done | bytes 1048608 | tf_op jit(solution)/shard_map/ppermute | solution.py:72
  72.9 2.4 constant_dynamic-update-slice_fusion.7
  76.3 1.1 constant_dynamic-update-slice_fusion.5
  77.4 1.1 constant_dynamic-update-slice_fusion.4
  78.5 2.4 constant_dynamic-update-slice_fusion.3
  80.9 1.1 constant_dynamic-update-slice_fusion.2
  82.0 1.1 constant_dynamic-update-slice_fusion.1
  83.1 1.1 constant_dynamic-update-slice_fusion
  84.3 6.1 %fusion.27 = (f32[512]{0:T(512)S(1)}, f32[512]{0:T(512)S(1)}, f32[512,2048]{1,0:T(8,128)S(1)}) fusion(bf16[512,1024]{0,1:T(8,128)(2,1)} %all-gather.5.cloned.1.call-done, bf16[1024,4096]{1,0:T(8,128)(2,1)} %constant_dynamic-update-slice_fusion, s32[]{:T(128)S(6)} %select_n.32, bf16[512,2048]{1,0:T(8,128)(2,1)} %param.16), kind=kOutput, calls=%fused_computation.63 | convolution fusion | flops 2152725504 | bytes 11538436 | tf_op jit(solution)/shard_map/dot_general | solution.py:76
  91.1 68.2 %all-gather.7.cloned.1.call-done = bf16[2048,1536]{1,0:T(8,128)(2,1)} async-done(((bf16[512,1536]{1,0:T(8,128)(2,1)}), bf16[2048,1536]{1,0:T(8,128)(2,1)}) %all-gather.7.cloned.1.call-update) | async-done | bytes 6291472 | tf_op jit(solution)/shard_map/all_gather | solution.py:87
  159.2 6.2 %convolution_convert_fusion.2 = bf16[512,1536]{1,0:T(8,128)(2,1)S(1)} fusion(bf16[512,2048]{1,0:T(8,128)(2,1)S(1)} %multiply_convert_fusion, bf16[2048,1536]{1,0:T(8,128)(2,1)} %all-gather.7.cloned.1.call-done), kind=kOutput, calls=%fused_computation.11 | convolution fusion | flops 3222011904 | bytes 9961472 | tf_op jit(solution)/shard_map/dot_general | solution.py:85
  165.5 1.3 collective-permute-start.5
  166.8 1.5 collective-permute-start.6
  168.3 106.1 %all-gather.11.cloned.1.call-done = bf16[1536,2048]{1,0:T(8,128)(2,1)} async-done(((bf16[1536,512]{1,0:T(8,128)(2,1)}), bf16[1536,2048]{1,0:T(8,128)(2,1)}) %all-gather.11.cloned.1.call-update) | async-done | bytes 6291472 | tf_op jit(solution)/shard_map/all_gather | solution.py:103
  274.4 114.9 %all-gather.9.cloned.1.call-done = bf16[2048,1536]{1,0:T(8,128)(2,1)} async-done(((bf16[512,1536]{1,0:T(8,128)(2,1)}), bf16[2048,1536]{1,0:T(8,128)(2,1)}) %all-gather.9.cloned.1.call-update) | async-done | bytes 6291472 | tf_op jit(solution)/shard_map/all_gather | solution.py:92
  389.4 15.3 %convolution_convert_fusion = bf16[512,2048]{1,0:T(8,128)(2,1)} fusion(bf16[1536,2048]{1,0:T(8,128)(2,1)} %all-gather.11.cloned.1.call-done, bf16[512,1536]{1,0:T(8,128)(2,1)} %copy-done.5, bf16[1,1536]{1,0:T(2,128)(2,1)S(1)} %collective-permute-done.6, bf16[1,1536]{1,0:T(2,128)(2,1)S(1)} %collective-permute-done.5, f32[1536]{0:T(1024)S(1)} %get-tuple-element.8, ...), kind=kOutput, calls=%fused_computation.9 | convolution fusion | flops 6461587456 | bytes 18380800 | tf_op jit(solution)/shard_map/dot_general | solution.py:102
  404.7 29.5 %reduce-scatter.2.cloned.1.call-done = bf16[512,512]{1,0:T(8,128)(2,1)} async-done(((bf16[512,2048]{1,0:T(8,128)(2,1)}), bf16[512,512]{1,0:T(8,128)(2,1)}) %reduce-scatter.2.cloned.1.call-update) | async-done | bytes 524304 | tf_op jit(solution)/shard_map/reduce_scatter | solution.py:105
  434.2 2.0 add_convert_fusion
  (47 shorter events, 7.5 us)
Async XLA Ops:
  6.5 12.2 %copy-start = (bf16[512,256]{1,0:T(8,128)(2,1)S(1)}, bf16[512,256]{1,0:T(8,128)(2,1)}, u32[]{:S(2)}) copy-start(bf16[512,256]{1,0:T(8,128)(2,1)} %param.12) | copy-start | bytes 786436
  6.5 77.7 %all-gather.5.cloned.1.call-start = ((), (), s32[]{:S(2)}) async-start(), calls=%async_computation.1 | async-start | bytes 1310720 | tf_op jit(solution)/shard_map/all_gather | solution.py:64
  6.5 13.0 %copy-start.4 = (f32[2]{0:T(128)S(1)}, f32[2]{0:T(128)}, u32[]{:S(2)}) copy-start(f32[2]{0:T(128)} %param.15) | copy-start | bytes 28
  7.6 7.1 %collective-permute-start = (bf16[2,128,128]{2,1,0:T(8,128)(2,1)S(1)}, bf16[2,128,128]{2,1,0:T(8,128)(2,1)S(1)}, u32[]{:S(2)}, u32[]{:S(2)}) collective-permute-start(bf16[2,128,128]{2,1,0:T(8,128)(2,1)S(1)} %get-tuple-element.12), channel_id=1, source_target_pairs={{0,4},{4,8},{8,12},{1,5},{5,9},{9,13},{2,6},{6,10},{10,14},{3,7},{... | collective-permute-start | bytes 196616 | tf_op jit(solution)/shard_map/ppermute | solution.py:22
  12.6 6.2 %collective-permute-start.1 = (bf16[2,128,128]{2,1,0:T(8,128)(2,1)S(1)}, bf16[2,128,128]{2,1,0:T(8,128)(2,1)S(1)}, u32[]{:S(2)}, u32[]{:S(2)}) collective-permute-start(bf16[2,128,128]{2,1,0:T(8,128)(2,1)S(1)} %get-tuple-element.13), channel_id=1, source_target_pairs={{4,0},{8,4},{12,8},{5,1},{9,5},{13,9},{6,2},{10,6},{14,10},{7,3},{... | collective-permute-start | bytes 196616 | tf_op jit(solution)/shard_map/ppermute | solution.py:24
  22.3 2.1 copy-start.1
  22.3 136.9 %all-gather.7.cloned.1.call-start = ((), (), s32[]{:S(2)}) async-start(), calls=%async_computation.2 | async-start | bytes 7864320 | tf_op jit(solution)/shard_map/all_gather | solution.py:87
  23.1 251.4 %all-gather.11.cloned.1.call-start = ((), (), s32[]{:S(2)}) async-start(), calls=%async_computation.4 | async-start | bytes 7864320 | tf_op jit(solution)/shard_map/all_gather | solution.py:103
  23.8 365.6 %all-gather.9.cloned.1.call-start = ((), (), s32[]{:S(2)}) async-start(), calls=%async_computation.3 | async-start | bytes 7864320 | tf_op jit(solution)/shard_map/all_gather | solution.py:92
  24.4 409.9 %reduce-scatter.2.cloned.1.call-start = ((), (), s32[]{:S(2)}) async-start(), calls=%async_computation.5 | async-start | bytes 2621440 | tf_op jit(solution)/shard_map/reduce_scatter | solution.py:105
  24.4 19.9 %collective-permute-start.2 = (bf16[1024,512]{1,0:T(8,128)(2,1)S(1)}, bf16[1024,512]{1,0:T(8,128)(2,1)S(1)}, u32[]{:S(2)}, u32[]{:S(2)}) collective-permute-start(bf16[1024,512]{1,0:T(8,128)(2,1)S(1)} %copy-done.1), channel_id=1, source_target_pairs={{0,1},{1,2},{2,3},{3,0},{4,5},{5,6},{6,7},{7,4},{8,9},{9,10},{10,1... | collective-permute-start | bytes 3145736 | tf_op jit(solution)/shard_map/ppermute | solution.py:72
  44.3 14.2 %collective-permute-start.3 = (bf16[1024,512]{1,0:T(8,128)(2,1)S(1)}, bf16[1024,512]{1,0:T(8,128)(2,1)S(1)}, u32[]{:S(2)}, u32[]{:S(2)}) collective-permute-start(bf16[1024,512]{1,0:T(8,128)(2,1)S(1)} %collective-permute-done.2), channel_id=1, source_target_pairs={{0,1},{1,2},{2,3},{3,0},{4,5},{5,6},{6,7},{7,4},{8,9},{9,10},{10,1... | collective-permute-start | bytes 3145736 | tf_op jit(solution)/shard_map/ppermute | solution.py:72
  58.5 14.3 %collective-permute-start.4 = (bf16[1024,512]{1,0:T(8,128)(2,1)S(1)}, bf16[1024,512]{1,0:T(8,128)(2,1)}, u32[]{:S(2)}, u32[]{:S(2)}) collective-permute-start(bf16[1024,512]{1,0:T(8,128)(2,1)S(1)} %collective-permute-done.3), channel_id=1, source_target_pairs={{0,1},{1,2},{2,3},{3,0},{4,5},{5,6},{6,7},{7,4},{8,9},{9,10},{10,1... | collective-permute-start | bytes 3145736 | tf_op jit(solution)/shard_map/ppermute | solution.py:72
  84.3 6.1 %copy-start.3 = (f32[2048]{0:T(1024)S(1)}, f32[2048]{0:T(1024)}, u32[]{:S(2)}) copy-start(f32[2048]{0:T(1024)} %param.18) | copy-start | bytes 24580
  91.0 77.2 %copy-start.2 = (f32[3,1536]{1,0:T(4,128)S(1)}, f32[3,1536]{1,0:T(4,128)}, u32[]{:S(2)}) copy-start(f32[3,1536]{1,0:T(4,128)} %param.21) | copy-start | bytes 55300
  91.0 298.3 %copy-start.6 = (f32[1536]{0:T(1024)S(1)}, f32[1536]{0:T(1024)}, u32[]{:S(2)}) copy-start(f32[1536]{0:T(1024)} %param.22) | copy-start | bytes 18436
  165.4 2.8 copy-start.5
  165.5 223.9 %collective-permute-start.5 = (bf16[1,1536]{1,0:T(2,128)(2,1)S(1)}, bf16[1,1536]{1,0:T(2,128)(2,1)S(1)}, u32[]{:S(2)}, u32[]{:S(2)}) collective-permute-start(bf16[1,1536]{1,0:T(2,128)(2,1)S(1)} %get-tuple-element.10), channel_id=1, source_target_pairs={{0,4},{4,8},{8,12},{1,5},{5,9},{9,13},{2,6},{6,10},{10,14},{3,7},{... | collective-permute-start | bytes 9224 | tf_op jit(solution)/shard_map/ppermute | solution.py:22
  166.8 222.6 %collective-permute-start.6 = (bf16[1,1536]{1,0:T(2,128)(2,1)S(1)}, bf16[1,1536]{1,0:T(2,128)(2,1)S(1)}, u32[]{:S(2)}, u32[]{:S(2)}) collective-permute-start(bf16[1,1536]{1,0:T(2,128)(2,1)S(1)} %get-tuple-element.11), channel_id=1, source_target_pairs={{4,0},{8,4},{12,8},{5,1},{9,5},{13,9},{6,2},{10,6},{14,10},{7,3},{... | collective-permute-start | bytes 9224 | tf_op jit(solution)/shard_map/ppermute | solution.py:24
Sparse Core Ops, SparseCore 0:
  22.4 19.8 all-gather.4
  43.9 115.3 all-gather.6
  160.8 113.5 all-gather.10
  275.9 113.4 all-gather.8
  404.8 29.3 reduce-scatter.1
